TPU v7x, 32 devices: a whole 2x2x4 slice. The times are simulated.
32 devices in a mesh: grp: 2 (over y), sp: 4 (over z), fs: 2 (over x), tp: 2 (over core).
Axes of the slice: x: 2, y: 2, z: 4, core: 2. Of those that a mesh axis runs over, the one named last changes fastest.
Arguments:
- tokens: bfloat16 [2, 6144, 2048], P('fs', ('grp', 'sp'), 'tp'), parts along dimension 1, may hold values from -12 to 12
- norm_gain: float32 [2048], replicated, may hold values from 0.1 to 1.9
- query_weight: bfloat16 [2048, 16, 64], P(None, 'tp'), may hold values from -3 to 3
- key_weight: bfloat16 [2048, 4, 64], P(None, 'tp'), may hold values from -3 to 3
- value_weight: bfloat16 [2048, 4, 64], P(None, 'tp'), may hold values from -0.125 to 0.125
- sink_logit: float32 [16], P('tp'), may hold values from 1 to 6
- pool_weight: bfloat16 [2048, 4, 256], P(None, None, 'tp'), may hold values from -0.125 to 0.125
- attn_out_weight: bfloat16 [16, 64, 2048], P('tp'), may hold values from -0.5 to 0.5
- pool_out_weight: bfloat16 [4, 256, 2048], P(None, 'tp'), may hold values from -0.1875 to 0.1875
Outputs:
- mixed: bfloat16 [2, 6144, 2048], P('fs', ('grp', 'sp', 'tp')), parts along dimension 1
There are 2 independent parts, one for each index of `grp`. A program takes and returns all parts, laid end to end along the dimension named above; an argument that names none is the same for every part. Nothing has to cross between parts.
All inputs are finite; a program needn't handle non-finite values.
Results may differ from a plain program's by a relative error of at most 0.0095.
The roundings to bfloat16 on the way count: a program that leaves them out, or rounds other values in their place, can miss the bound.
Values may be sent and summed in bfloat16 or wider, within the bound.
No kernel may reach another device: no remote copies, remote signals or barrier semaphores. Data moves between devices by JAX's collectives and lax.ppermute only.
A program may use at most 128 MiB of HBM per device.

v0:
```python
import jax
import jax.numpy as jnp
from jax import lax
from jax.sharding import PartitionSpec as P

WINDOW = 128


def from_behind(value, axis, steps):
    count = lax.axis_size(axis)
    first, last = (max(0, -steps), min(count, count - steps))
    return lax.ppermute(value, axis, [(source, source + steps) for source in range(first, last)])


def rms_norm(rows, gain):
    values = rows.astype(jnp.float32)
    scale = lax.rsqrt(jnp.mean(values * values, axis=-1, keepdims=True) + 1e-06)
    return (values * scale * gain).astype(jnp.bfloat16)


def attend(query, key, value, key_tail, value_tail, sinks, offset):
    rows = query.shape[0]
    local_kv = key_tail.shape[1]
    head_dim = key_tail.shape[2]
    group = query.shape[1] // (local_kv * head_dim)
    blocks = rows // WINDOW
    qb = query.reshape(blocks, WINDOW, local_kv, group, head_dim)

    def banded(tensor, tail):
        tb = tensor.reshape(blocks, WINDOW, local_kv, head_dim)
        whole = jnp.concatenate([tail, tensor.reshape(rows, local_kv, head_dim)], axis=0)
        before = whole[:rows].reshape(blocks, WINDOW, local_kv, head_dim)
        return jnp.concatenate([before, tb], axis=1)

    kw = banded(key, key_tail)
    vw = banded(value, value_tail)
    qi = jnp.arange(WINDOW, dtype=jnp.int32)[:, None]
    kj = jnp.arange(2 * WINDOW, dtype=jnp.int32)[None, :]
    dist = WINDOW + qi - kj
    inside = (dist >= 0) & (dist < WINDOW)
    key_pos = (
        offset + jnp.arange(blocks, dtype=jnp.int32)[:, None, None] * WINDOW - WINDOW + kj[None]
    )
    mask = inside[None] & (key_pos >= 0)
    scores = jnp.einsum(
        "nqhgd,nkhd->nhgqk", qb, kw, preferred_element_type=jnp.float32
    ) * head_dim ** (-0.5)
    scores = jnp.where(mask[:, None, None], scores, -jnp.inf)
    sink = sinks.reshape(1, local_kv, group, 1, 1)
    top = jnp.maximum(jnp.max(scores, axis=-1, keepdims=True), sink)
    expo = jnp.exp(scores - top)
    total = jnp.sum(expo, axis=-1, keepdims=True) + jnp.exp(sink - top)
    weight = (expo / total).astype(jnp.bfloat16)
    out = jnp.einsum("nhgqk,nkhd->nqhgd", weight, vw, preferred_element_type=jnp.float32)
    return out.reshape(rows, -1).astype(jnp.bfloat16)


def shards(
    tokens,
    norm_gain,
    query_weight,
    key_weight,
    value_weight,
    sink_logit,
    pool_weight,
    attn_out_weight,
    pool_out_weight,
):
    whole = lax.all_gather(tokens, "tp", axis=2, tiled=True)[0]
    rows = whole.shape[0]
    width = whole.shape[1]
    local_kv = key_weight.shape[1]
    head_dim = key_weight.shape[2]
    channels = pool_weight.shape[2]
    normed = rms_norm(whole, norm_gain)
    query = jnp.dot(
        normed, query_weight.reshape(width, -1), preferred_element_type=jnp.float32
    ).astype(jnp.bfloat16)
    key = jnp.dot(normed, key_weight.reshape(width, -1), preferred_element_type=jnp.float32).astype(
        jnp.bfloat16
    )
    value = jnp.dot(
        normed, value_weight.reshape(width, -1), preferred_element_type=jnp.float32
    ).astype(jnp.bfloat16)
    pooled_in = jnp.dot(
        normed, pool_weight.reshape(width, -1), preferred_element_type=jnp.float32
    ).astype(jnp.bfloat16)
    pool_rows = pooled_in.reshape(rows, 4, channels)
    key_rows = key.reshape(rows, local_kv, head_dim)
    value_rows = value.reshape(rows, local_kv, head_dim)
    key_tail, value_tail, pool_tail = from_behind(
        (key_rows[rows - WINDOW :], value_rows[rows - WINDOW :], pool_rows[rows - WINDOW :]),
        "sp",
        1,
    )
    offset = lax.axis_index("sp") * rows
    attended = attend(query, key, value, key_tail, value_tail, sink_logit, offset)
    prefix_total = jnp.sum(pool_rows[:, 3].astype(jnp.float32), axis=0)
    totals = lax.all_gather(prefix_total[None], "sp", axis=0, tiled=True)
    below = jnp.arange(totals.shape[0], dtype=jnp.int32) < lax.axis_index("sp")
    carried = jnp.sum(jnp.where(below[:, None], totals, 0.0), axis=0)
    reaches = jnp.array([2.0, 4.0, 16.0, 1000000000.0], jnp.float32)
    ext = jnp.concatenate([pool_tail, pool_rows], axis=0)
    position = jnp.arange(rows, dtype=jnp.int32)[:, None]
    source = jnp.arange(rows + WINDOW, dtype=jnp.int32)[None, :]
    gap = (position + WINDOW - source).astype(jnp.float32)
    group_ids = jnp.arange(4, dtype=jnp.int32)[:, None, None]
    band = (
        (gap[None] >= 0.0)
        & (gap[None] < reaches[:, None, None])
        & ((group_ids < 3) | (source[None] >= WINDOW))
    )
    sums = jnp.einsum(
        "gij,jgc->igc", band.astype(jnp.bfloat16), ext, preferred_element_type=jnp.float32
    )
    carry_rows = jnp.concatenate([jnp.zeros((3, channels), jnp.float32), carried[None]], axis=0)
    sums = sums + carry_rows[None]
    count = (offset + jnp.arange(1, rows + 1, dtype=jnp.int32)).astype(jnp.float32)
    denom = jnp.minimum(count[:, None], reaches[None, :])[:, :, None]
    pooled = (
        (sums / denom - pool_rows.astype(jnp.float32))
        .astype(jnp.bfloat16)
        .reshape(rows, 4 * channels)
    )
    attn_rows = attn_out_weight.reshape(-1, width)
    pool_weight_rows = pool_out_weight.reshape(-1, width)
    part_sum = jnp.dot(attended, attn_rows, preferred_element_type=jnp.float32)
    result = lax.psum_scatter(
        (part_sum + jnp.dot(pooled, pool_weight_rows, preferred_element_type=jnp.float32)).astype(
            jnp.bfloat16
        ),
        "tp",
        scatter_dimension=0,
        tiled=True,
    )
    return result[None]


def solution(mesh):
    in_specs = (
        P("fs", ("grp", "sp"), "tp"),
        P(),
        P(None, "tp", None),
        P(None, "tp", None),
        P(None, "tp", None),
        P("tp"),
        P(None, None, "tp"),
        P("tp", None, None),
        P(None, "tp", None),
    )
    out_specs = P("fs", ("grp", "sp", "tp"), None)
    return jax.shard_map(shards, mesh=mesh, in_specs=in_specs, out_specs=out_specs, check_vma=False)
```

profile of v0, /device:TPU:0, one launch (start us, length us, event | category | flops | bytes accessed | tf_op | source)
XLA Modules:
  0.0 103.8 jit_solution(3450044622372322319)
XLA Ops:
  6.5 0.0 all-gather.4.cloned.1.call-start
  6.5 0.7 all-gather.4.cloned.1.call-update
  7.3 0.0 reduce-scatter.2.cloned.1.call-start
  7.3 0.7 max.18
  8.1 0.1 add_compare_fusion
  8.2 0.7 broadcast_or_fusion
  8.8 0.7 broadcast_minimum_fusion
  9.6 0.3 broadcast_and_fusion
  9.9 0.0 copy-start.10
  9.9 1.5 %broadcast_compare_fusion = pred[768,896]{1,0:T(8,128)(4,1)} fusion(s32[768]{0:T(1024)S(1)} %iota_add_fusion), kind=kLoop, calls=%fused_computation.34 | loop fusion | flops 2064384 | bytes 691200 | tf_op jit(solution)/shard_map/ge | solution.py:109
  11.4 1.8 %subtract_convert_fusion = f32[768,896]{1,0:T(8,128)} fusion(s32[768]{0:T(1024)S(1)} %iota_add_fusion), kind=kLoop, calls=%fused_computation.22 | loop fusion | flops 1376256 | bytes 2755584 | tf_op jit(solution)/shard_map/convert_element_type | solution.py:106
  13.1 10.6 %all-gather.4.cloned.1.call-done = bf16[1,768,2048]{2,1,0:T(8,128)(2,1)} async-done(((bf16[1,768,1024]{2,1,0:T(8,128)(2,1)}), bf16[1,768,2048]{2,1,0:T(8,128)(2,1)}) %all-gather.4.cloned.1.call-update) | async-done | bytes 3145744 | tf_op jit(solution)/shard_map/all_gather | solution.py:69
  23.8 2.7 %fusion.4 = f32[768]{0:T(1024)S(1)} fusion(bf16[1,768,2048]{2,1,0:T(8,128)(2,1)} %all-gather.4.cloned.1.call-done), kind=kLoop, calls=%fused_computation.6 | loop fusion | flops 4717824 | bytes 3148800 | tf_op jit(solution)/shard_map/reduce_sum | solution.py:17
  26.5 0.1 copy-done.1
  26.6 2.3 %convolution_convert_fusion.2 = bf16[768,128]{0,1:T(8,128)(2,1)S(1)} fusion(bf16[2048,128]{0,1:T(8,128)(2,1)} %bitcast.105, bf16[1,768,2048]{2,1,0:T(8,128)(2,1)S(1)} %copy-done.1, f32[2048]{0:T(1024)S(1)} %copy-done.10, f32[768]{0:T(1024)S(1)} %add_rsqrt_fusion), kind=kOutput, calls=%fused_computation.37 | convolution fusion | flops 409042944 | bytes 3877888 | tf_op jit(solution)/shard_map/dot_general | solution.py:82
  28.9 0.2 reshape.317
  29.2 0.0 copy-start.2
  29.2 0.0 copy-start.8
  29.2 3.4 %convolution_convert_fusion.1 = bf16[768,128]{0,1:T(8,128)(2,1)S(1)} fusion(bf16[2048,128]{0,1:T(8,128)(2,1)} %bitcast.106, bf16[1,768,2048]{2,1,0:T(8,128)(2,1)} %all-gather.4.cloned.1.call-done, f32[2048]{0:T(1024)S(1)} %copy-done.10, f32[768]{0:T(1024)S(1)} %add_rsqrt_fusion), kind=kOutput, calls=%fused_computation.36 | convolution fusion | flops 409042944 | bytes 3877888 | tf_op jit(solution)/shard_map/dot_general | solution.py:79
  32.6 4.3 %collective-permute-start.1 = (bf16[128,2,64]{0,2,1:T(8,128)(2,1)S(1)}, bf16[128,2,64]{0,2,1:T(8,128)(2,1)}, u32[]{:S(2)}, u32[]{:S(2)}) collective-permute-start(bf16[128,2,64]{0,2,1:T(8,128)(2,1)S(1)} %bitcast.99), channel_id=1, source_target_pairs={{0,4},{4,8},{8,12},{1,5},{5,9},{9,13},{2,6},{6,10},{10,14},{3,7},{... | collective-permute-start | bytes 98312 | tf_op jit(solution)/shard_map/ppermute | solution.py:12
  36.9 3.4 %collective-permute-start = (bf16[128,2,64]{0,2,1:T(8,128)(2,1)S(1)}, bf16[128,2,64]{0,2,1:T(8,128)(2,1)}, u32[]{:S(2)}, u32[]{:S(2)}) collective-permute-start(bf16[128,2,64]{0,2,1:T(8,128)(2,1)S(1)} %bitcast.98), channel_id=1, source_target_pairs={{0,4},{4,8},{8,12},{1,5},{5,9},{9,13},{2,6},{6,10},{10,14},{3,7},{... | collective-permute-start | bytes 98312 | tf_op jit(solution)/shard_map/ppermute | solution.py:12
  40.3 0.0 copy-start.9
  40.3 2.0 %fusion.25 = bf16[768,512]{0,1:T(8,128)(2,1)S(1)} fusion(bf16[256,8,4,128]{3,2,1,0:T(4,128)(2,1)S(1)} %bitcast.103, bf16[1,768,2048]{2,1,0:T(8,128)(2,1)S(1)} %copy-done.2, f32[2048]{0:T(1024)S(1)} %copy-done.10, f32[768]{0:T(1024)S(1)} %add_rsqrt_fusion), kind=kOutput, calls=%fused_computation.31 | convolution fusion | flops 1617297408 | bytes 6040576 | tf_op jit(solution)/shard_map/dot_general | solution.py:85
  42.4 0.1 convert_reduce_fusion
  42.5 8.5 %all-gather.1 = f32[4,1,128]{2,1,0:T(1,128)S(1)} all-gather(f32[1,1,128]{2,1,0:T(1,128)S(1)} %bitcast.101), channel_id=2, replica_groups=mesh['grp'=2,'sp'=4,'fs'=2,'tp'=2] {'sp'}, dimensions={0}, use_global_device_ids=true | all-gather | bytes 2560 | tf_op jit(solution)/shard_map/all_gather | solution.py:99
  50.9 3.7 %collective-permute-start.2 = (bf16[128,4,128]{0,2,1:T(8,128)(2,1)S(1)}, bf16[128,4,128]{0,2,1:T(8,128)(2,1)}, u32[]{:S(2)}, u32[]{:S(2)}) collective-permute-start(bf16[128,4,128]{0,2,1:T(8,128)(2,1)S(1)} %bitcast.97), channel_id=1, source_target_pairs={{0,4},{4,8},{8,12},{1,5},{5,9},{9,13},{2,6},{6,10},{10,14},{3,7},{... | collective-permute-start | bytes 393224 | tf_op jit(solution)/shard_map/ppermute | solution.py:12
  54.6 0.0 copy-done.9
  54.6 2.7 %convolution_convert_fusion = bf16[768,512]{1,0:T(8,128)(2,1)} fusion(bf16[2048,512]{0,1:T(8,128)(2,1)S(1)} %bitcast.104, bf16[1,768,2048]{2,1,0:T(8,128)(2,1)S(1)} %copy-done.2, f32[2048]{0:T(1024)S(1)} %copy-done.10, f32[768]{0:T(1024)S(1)} %add_rsqrt_fusion), kind=kOutput, calls=%fused_computation.32 | convolution fusion | flops 1617297408 | bytes 6040576 | tf_op jit(solution)/shard_map/dot_general | solution.py:76
  57.4 0.7 select_reduce_fusion
  58.0 0.2 reshape.321
  58.3 3.6 %reshape.334 = bf16[6,128,2,4,64]{4,3,2,1,0:T(4,128)(2,1)} reshape(bf16[768,512]{1,0:T(8,128)(2,1)} %convolution_convert_fusion) | data formatting | bytes 1572864 | tf_op jit(solution)/shard_map/reshape | solution.py:27
  61.9 1.3 %concatenate.23 = f32[4,128]{1,0:T(4,128)} pad(f32[1,128]{1,0:T(1,128)} %bitcast.102, f32[]{:T(128)} %constant.14.clone.1), padding=3_0x0_0 | pad | bytes 2564 | tf_op jit(solution)/shard_map/concatenate | solution.py:116
  63.2 0.0 collective-permute-done.1
  63.2 0.8 copy_bitcast_fusion
  64.0 2.7 %fusion.13 = (f32[6,2,4,128]{3,2,1,0:T(4,128)S(1)}, f32[6,2,256,128,4]{3,2,4,1,0:T(8,128)S(1)}) fusion(pred[6,128,256]{1,2,0:T(8,128)(4,1)S(1)} %broadcast_and_fusion, bf16[6,128,2,4,64]{4,3,2,1,0:T(4,128)(2,1)} %reshape.334, bf16[6,128,2,64]{1,3,2,0:T(8,128)(2,1)S(1)} %copy.28, bf16[6,128,2,64]{1,3,2,0:T(8,128)(2,1)S(1)} %copy_bitcast_fusion), kind=kOutput, calls=%fused_computation.19 | convolution fusion | flops 206825472 | bytes 7692288 | tf_op jit(solution)/shard_map/nqhgd,nkhd->nhgqk/dot_general | solution.py:45
  66.7 0.1 broadcast_maximum_fusion
  66.8 1.7 %fusion.8 = f32[6,2,4,128]{3,2,1,0:T(4,128)S(1)} fusion(f32[6,2,256,128,4]{3,2,4,1,0:T(8,128)S(1)} %get-tuple-element.6, f32[6,2,4,128]{3,2,1,0:T(4,128)S(1)} %broadcast_maximum_fusion, pred[6,128,256]{1,2,0:T(8,128)(4,1)S(1)} %broadcast_and_fusion), kind=kLoop, calls=%fused_computation.14 | loop fusion | flops 6285312 | bytes 6537216 | tf_op jit(solution)/shard_map/reduce_sum | solution.py:52
  68.4 0.1 exponential_add_fusion
  68.5 0.0 collective-permute-done
  68.5 0.8 copy_bitcast_fusion.1
  69.3 1.7 %fusion.31 = bf16[6,128,2,4,64]{1,4,3,2,0:T(8,128)(2,1)S(1)} fusion(f32[6,2,256,128,4]{3,2,4,1,0:T(8,128)S(1)} %get-tuple-element.6, f32[6,2,4,128]{3,2,1,0:T(4,128)S(1)} %exponential_add_fusion, f32[6,2,4,128]{3,2,1,0:T(4,128)S(1)} %broadcast_maximum_fusion, pred[6,128,256]{1,2,0:T(8,128)(4,1)S(1)} %broadcast_and_fusion, ...), kind=kOutput, calls=%fused_computation.35 | convolution fusion | flops 210370560 | bytes 7716864 | tf_op jit(solution)/shard_map/nhgqk,nkhd->nqhgd/dot_general | solution.py:54
  71.1 0.6 copy.32
  71.7 0.0 copy-start.7
  71.7 4.5 %fusion.38 = f32[768,2048]{1,0:T(8,128)} fusion(bf16[512,2048]{1,0:T(8,128)(2,1)S(1)} %bitcast.91, bf16[64,8,6,128]{3,2,1,0:T(8,128)(2,1)S(1)} %bitcast.92), kind=kOutput, calls=%fused_computation.41 | convolution fusion | flops 1610612736 | bytes 9175040 | tf_op jit(solution)/shard_map/dot_general | solution.py:127
  76.2 0.0 collective-permute-done.2
  76.2 11.3 %fusion.7 = bf16[768,2048]{1,0:T(8,128)(2,1)} fusion(f32[768,2048]{1,0:T(8,128)} %fusion.38, bf16[4,128,2048]{2,1,0:T(8,128)(2,1)} %param.18, bf16[768,4,128]{0,2,1:T(8,128)(2,1)} %bitcast.96, f32[768,896]{1,0:T(8,128)} %subtract_convert_fusion, f32[4]{0:T(128)S(1)} %copy-done.7, pred[4,896]{1,0:T(4,128)(4,1)S(1)} %copy-done.5, ...), kind=kOutput, calls=%fused_computation.10 | convolution fusion | flops 2330460160 | bytes 15910416 | tf_op jit(solution)/shard_map/dot_general | solution.py:129
  87.5 0.0 reduce-scatter.2.cloned.1.call-update
  87.5 9.5 %reduce-scatter.2.cloned.1.call-done = bf16[384,2048]{1,0:T(8,128)(2,1)} async-done(((bf16[768,2048]{1,0:T(8,128)(2,1)}), bf16[384,2048]{1,0:T(8,128)(2,1)}) %reduce-scatter.2.cloned.1.call-update) | async-done | bytes 1572880 | tf_op jit(solution)/shard_map/reduce_scatter | solution.py:128
  (29 shorter events, 0.2 us)
Async XLA Ops:
  6.5 65.1 %copy-start = (bf16[8,64,2048]{2,1,0:T(8,128)(2,1)S(1)}, bf16[8,64,2048]{2,1,0:T(8,128)(2,1)}, u32[]{:S(2)}) copy-start(bf16[8,64,2048]{2,1,0:T(8,128)(2,1)} %param.17) | copy-start | bytes 6291460
  6.5 17.2 %all-gather.4.cloned.1.call-start = ((), (), s32[]{:S(2)}) async-start(), calls=%async_computation.1 | async-start | bytes 4718592 | tf_op jit(solution)/shard_map/all_gather | solution.py:69
  7.3 89.7 %reduce-scatter.2.cloned.1.call-start = ((), (), s32[]{:S(2)}) async-start(), calls=%async_computation.2 | async-start | bytes 4718592 | tf_op jit(solution)/shard_map/reduce_scatter | solution.py:128
  9.9 16.6 %copy-start.10 = (f32[2048]{0:T(1024)S(1)}, f32[2048]{0:T(1024)}, u32[]{:S(2)}) copy-start(f32[2048]{0:T(1024)} %param.11) | copy-start | bytes 24580
  23.8 2.8 %copy-start.1 = (bf16[1,768,2048]{2,1,0:T(8,128)(2,1)S(1)}, bf16[1,768,2048]{2,1,0:T(8,128)(2,1)}, u32[]{:S(2)}) copy-start(bf16[1,768,2048]{2,1,0:T(8,128)(2,1)} %all-gather.4.cloned.1.call-done) | copy-start | bytes 9437188
  29.2 11.1 %copy-start.2 = (bf16[1,768,2048]{2,1,0:T(8,128)(2,1)S(1)}, bf16[1,768,2048]{2,1,0:T(8,128)(2,1)}, u32[]{:S(2)}) copy-start(bf16[1,768,2048]{2,1,0:T(8,128)(2,1)} %all-gather.4.cloned.1.call-done) | copy-start | bytes 9437188
  29.2 11.1 %copy-start.8 = (bf16[2048,4,128]{2,1,0:T(4,128)(2,1)S(1)}, bf16[2048,4,128]{2,1,0:T(4,128)(2,1)}, u32[]{:S(2)}) copy-start(bf16[2048,4,128]{2,1,0:T(4,128)(2,1)} %param.16) | copy-start | bytes 6291460
  32.6 30.6 %collective-permute-start.1 = (bf16[128,2,64]{0,2,1:T(8,128)(2,1)S(1)}, bf16[128,2,64]{0,2,1:T(8,128)(2,1)}, u32[]{:S(2)}, u32[]{:S(2)}) collective-permute-start(bf16[128,2,64]{0,2,1:T(8,128)(2,1)S(1)} %bitcast.99), channel_id=1, source_target_pairs={{0,4},{4,8},{8,12},{1,5},{5,9},{9,13},{2,6},{6,10},{10,14},{3,7},{... | collective-permute-start | bytes 98312 | tf_op jit(solution)/shard_map/ppermute | solution.py:12
  36.9 31.7 %collective-permute-start = (bf16[128,2,64]{0,2,1:T(8,128)(2,1)S(1)}, bf16[128,2,64]{0,2,1:T(8,128)(2,1)}, u32[]{:S(2)}, u32[]{:S(2)}) collective-permute-start(bf16[128,2,64]{0,2,1:T(8,128)(2,1)S(1)} %bitcast.98), channel_id=1, source_target_pairs={{0,4},{4,8},{8,12},{1,5},{5,9},{9,13},{2,6},{6,10},{10,14},{3,7},{... | collective-permute-start | bytes 98312 | tf_op jit(solution)/shard_map/ppermute | solution.py:12
  40.3 14.3 %copy-start.9 = (bf16[2048,8,64]{0,2,1:T(8,128)(2,1)S(1)}, bf16[2048,8,64]{0,2,1:T(8,128)(2,1)}, u32[]{:S(2)}) copy-start(bf16[2048,8,64]{0,2,1:T(8,128)(2,1)} %param.12) | copy-start | bytes 6291460
  42.3 15.0 %copy-start.4 = (bf16[768,512]{0,1:T(8,128)(2,1)}, bf16[768,512]{0,1:T(8,128)(2,1)S(1)}, u32[]{:S(2)}) copy-start(bf16[768,512]{0,1:T(8,128)(2,1)S(1)} %fusion.25) | copy-start | bytes 2359300
  50.9 25.2 %collective-permute-start.2 = (bf16[128,4,128]{0,2,1:T(8,128)(2,1)S(1)}, bf16[128,4,128]{0,2,1:T(8,128)(2,1)}, u32[]{:S(2)}, u32[]{:S(2)}) collective-permute-start(bf16[128,4,128]{0,2,1:T(8,128)(2,1)S(1)} %bitcast.97), channel_id=1, source_target_pairs={{0,4},{4,8},{8,12},{1,5},{5,9},{9,13},{2,6},{6,10},{10,14},{3,7},{... | collective-permute-start | bytes 393224 | tf_op jit(solution)/shard_map/ppermute | solution.py:12
  71.6 4.5 %copy-start.3 = (pred[768,896]{1,0:T(8,128)(4,1)S(1)}, pred[768,896]{1,0:T(8,128)(4,1)}, u32[]{:S(2)}) copy-start(pred[768,896]{1,0:T(8,128)(4,1)} %broadcast_compare_fusion) | copy-start | bytes 2064388
  71.7 4.5 %copy-start.5 = (pred[4,896]{1,0:T(4,128)(4,1)S(1)}, pred[4,896]{1,0:T(4,128)(4,1)}, u32[]{:S(2)}) copy-start(pred[4,896]{1,0:T(4,128)(4,1)} %broadcast_or_fusion) | copy-start | bytes 10756
  71.7 4.5 %copy-start.6 = (f32[4,128]{1,0:T(4,128)S(1)}, f32[4,128]{1,0:T(4,128)}, u32[]{:S(2)}) copy-start(f32[4,128]{1,0:T(4,128)} %concatenate.23) | copy-start | bytes 6148
  71.7 4.5 %copy-start.7 = (f32[4]{0:T(128)S(1)}, f32[4]{0:T(128)}, u32[]{:S(2)}) copy-start(f32[4]{0:T(128)} %constant.13.clone) | copy-start | bytes 52
Sparse Core Ops, SparseCore 0:
  8.9 14.8 all-gather.3
  87.7 9.2 reduce-scatter.1
where the time goes:
time: 104 us
  matrix products  30.6 us (29%)
  waiting for transfers between devices  20.8 us (20%)
  between operations  13.7 us (13%)
  other arithmetic  12 us (12%)
  starting transfers between devices  11.4 us (11%)
  blocking collectives  8.46 us (8%)
  local copies, waits for them, and re-layouts  6.9 us (7%)
    ppermute x3, starting transfers between devices, from_behind(): lax.ppermute(value, axis, [(source, source + steps) for source in range(f...  11.3 us
    dot_general x1, matrix products, shards(): jnp.dot(pooled, pool_weight_rows, preferred_element_type=jnp.float32)  11.3 us
    all_gather x1, waiting for transfers between devices, shards(): whole = lax.all_gather(tokens, 'tp', axis=2, tiled=True)[0]  10.6 us
    reduce_scatter x1, waiting for transfers between devices, shards(): lax.psum_scatter((part_sum + jnp.dot(pooled, pool_weight_rows, preferred_...  9.46 us
    all_gather x1, blocking collectives, shards(): totals = lax.all_gather(prefix_total[None], 'sp', axis=0, tiled=True)  8.46 us
    dot_general x1, matrix products, shards(): part_sum = jnp.dot(attended, attn_rows, preferred_element_type=jnp.float32)  4.48 us
    reshape x1, local copies, waits for them, and re-layouts, attend(): qb = query.reshape(blocks, WINDOW, local_kv, group, head_dim)  3.63 us
    dot_general x1, matrix products, shards(): jnp.dot(normed, key_weight.reshape(width, -1), preferred_element_type=jnp...  3.38 us
  transfers between devices with their start and end apart: 5, of which 2 were waited for; matrix products, arithmetic and copies ran while one was open for 28% of the time, Pallas kernels for 0%

commit v1 on v0

--- a/solution.py
+++ b/solution.py
@@ -2,8 +2,12 @@
 import jax.numpy as jnp
 from jax import lax
 from jax.sharding import PartitionSpec as P
+from jax.lax import all_gather
 
 WINDOW = 128
+recover_set_here = lambda vector, group_axis, d0: jnp.concatenate(
+    all_gather(vector, group_axis), axis=d0
+)
 
 
 def from_behind(value, axis, steps):
@@ -66,7 +70,7 @@
     attn_out_weight,
     pool_out_weight,
 ):
-    whole = lax.all_gather(tokens, "tp", axis=2, tiled=True)[0]
+    whole = recover_set_here(tokens, "tp", 2)[0]
     rows = whole.shape[0]
     width = whole.shape[1]
     local_kv = key_weight.shape[1]

time: 104 us -> 111 us (1.067)
  local copies, waits for them, and re-layouts: 6.9 us -> 13.8 us
  other arithmetic: 12 us -> 13.2 us
  waiting for transfers between devices: 20.8 us -> 19.6 us
    all_gather x0 -> x1, local copies, waits for them, and re-layouts: none -> 4.63 us  [all_gather(vector, group_axis)]
    dot_general x1, matrix products: 2.32 us -> 0.59 us  [shards(): jnp.dot(normed, value_weight.reshape(width, -1), preferred_element_type=j...]
    dot_general x1, matrix products: 2.01 us -> 3.68 us  [shards(): jnp.dot(normed, pool_weight.reshape(width, -1), preferred_element_type=jn...]
    unnamed x22 -> x26, local copies, waits for them, and re-layouts: 0.14 us -> 1.79 us
    all_gather x1, waiting for transfers between devices: 10.6 us -> 9.43 us  [all_gather(vector, group_axis)]
  transfers between devices with their start and end apart: 5 -> 5, of which waited for: 2 -> 2; matrix products, arithmetic and copies ran while one was open for 28% -> 31% of each run, Pallas kernels for 0% -> 0%
where the time goes in v1:
time: 111 us; the launch traced here: 110 us
  matrix products  29.7 us (27%)
  waiting for transfers between devices  19.6 us (18%)
  local copies, waits for them, and re-layouts  13.8 us (12%)
  between operations  13.7 us (12%)
  other arithmetic  13.2 us (12%)
  starting transfers between devices  11.7 us (11%)
  blocking collectives  8.46 us (8%)
    ppermute x3, starting transfers between devices, from_behind(): lax.ppermute(value, axis, [(source, source + steps) for source in range(f...  11.6 us
    dot_general x1, matrix products, shards(): jnp.dot(pooled, pool_weight_rows, preferred_element_type=jnp.float32)  11.3 us
    reduce_scatter x1, waiting for transfers between devices, shards(): lax.psum_scatter((part_sum + jnp.dot(pooled, pool_weight_rows, preferred_...  9.46 us
    all_gather x1, waiting for transfers between devices, all_gather(vector, group_axis)  9.43 us
    all_gather x1, blocking collectives, shards(): totals = lax.all_gather(prefix_total[None], 'sp', axis=0, tiled=True)  8.46 us
    all_gather x1, local copies, waits for them, and re-layouts, all_gather(vector, group_axis)  4.63 us
    dot_general x1, matrix products, shards(): part_sum = jnp.dot(attended, attn_rows, preferred_element_type=jnp.float32)  4.49 us
    dot_general x1, matrix products, shards(): jnp.dot(normed, pool_weight.reshape(width, -1), preferred_element_type=jn...  3.68 us
  transfers between devices with their start and end apart: 5, of which 2 were waited for; matrix products, arithmetic and copies ran while one was open for 31% of the time, Pallas kernels for 0%

profile of v1, /device:TPU:0, one launch (start us, length us, event | category | flops | bytes accessed | tf_op | source)
XLA Modules:
  0.0 110.1 jit_solution(18215774276980217313)
XLA Ops:
  6.5 0.7 all-gather.5.cloned.1.call-update
  7.3 0.0 reduce-scatter.2.cloned.1.call-start
  7.3 0.7 max.18
  8.0 0.7 mul.56
  8.8 0.5 iota_compare_fusion.1
  9.3 0.1 add_compare_fusion
  9.4 0.7 broadcast_or_fusion
  10.1 0.7 broadcast_minimum_fusion
  10.8 0.3 broadcast_and_fusion
  11.1 1.5 %broadcast_compare_fusion = pred[768,896]{1,0:T(8,128)(4,1)} fusion(s32[768]{0:T(1024)S(1)} %iota_add_fusion), kind=kLoop, calls=%fused_computation.33 | loop fusion | flops 2064384 | bytes 691200 | tf_op jit(solution)/shard_map/ge | solution.py:113
  12.6 1.8 %subtract_convert_fusion = f32[768,896]{1,0:T(8,128)} fusion(s32[768]{0:T(1024)S(1)} %iota_add_fusion), kind=kLoop, calls=%fused_computation.21 | loop fusion | flops 1376256 | bytes 2755584 | tf_op jit(solution)/shard_map/convert_element_type | solution.py:110
  14.3 9.4 %all-gather.5.cloned.1.call-done = bf16[2,768,1024]{2,1,0:T(8,128)(2,1)} async-done(((bf16[1,768,1024]{2,1,0:T(8,128)(2,1)}), bf16[2,768,1024]{2,1,0:T(8,128)(2,1)}) %all-gather.5.cloned.1.call-update) | async-done | bytes 3145744 | tf_op jit(solution)/shard_map/all_gather | solution.py:9
  23.8 4.6 %copy.26 = bf16[2,768,1024]{1,2,0:T(8,128)(2,1)} copy(bf16[2,768,1024]{2,1,0:T(8,128)(2,1)} %all-gather.5.cloned.1.call-done) | data formatting | bytes 6291456 | tf_op jit(solution)/shard_map/all_gather | solution.py:9
  28.4 2.7 %fusion.4 = f32[768]{0:T(1024)S(1)} fusion(bf16[2,768,1024]{1,2,0:T(8,128)(2,1)} %copy.26), kind=kLoop, calls=%fused_computation.6 | loop fusion | flops 4717824 | bytes 3148800 | tf_op jit(solution)/shard_map/reduce_sum | solution.py:21
  31.1 0.1 copy-done.1
  31.2 0.8 fusion.6
  32.0 0.0 copy-start.6
  32.0 1.6 %copy-done.2 = bf16[2,1,768,1024]{2,3,0,1:T(8,128)(2,1)} copy-done((bf16[2,1,768,1024]{2,3,0,1:T(8,128)(2,1)}, bf16[2,1,768,1024]{2,3,0,1:T(8,128)(2,1)S(1)}, u32[]{:S(2)}) %copy-start.2) | copy-done | bytes 3145752
  33.7 0.6 convolution_convert_fusion.2
  34.3 0.2 reshape.316
  34.5 4.5 %collective-permute-start = (bf16[128,2,64]{0,2,1:T(8,128)(2,1)S(1)}, bf16[128,2,64]{0,2,1:T(8,128)(2,1)}, u32[]{:S(2)}, u32[]{:S(2)}) collective-permute-start(bf16[128,2,64]{0,2,1:T(8,128)(2,1)S(1)} %bitcast.109), channel_id=1, source_target_pairs={{0,4},{4,8},{8,12},{1,5},{5,9},{9,13},{2,6},{6,10},{10,14},{3,7},{... | collective-permute-start | bytes 98312 | tf_op jit(solution)/shard_map/ppermute | solution.py:16
  39.0 2.5 %convolution_convert_fusion.1 = bf16[768,128]{0,1:T(8,128)(2,1)S(1)} fusion(bf16[2048,128]{0,1:T(8,128)(2,1)S(1)} %bitcast.105, bf16[768,2048]{0,1:T(8,128)(2,1)} %bitcast.98), kind=kOutput, calls=%fused_computation.35 | convolution fusion | flops 402751488 | bytes 3866624 | tf_op jit(solution)/shard_map/dot_general | solution.py:83
  41.5 3.4 %collective-permute-start.1 = (bf16[128,2,64]{0,2,1:T(8,128)(2,1)S(1)}, bf16[128,2,64]{0,2,1:T(8,128)(2,1)}, u32[]{:S(2)}, u32[]{:S(2)}) collective-permute-start(bf16[128,2,64]{0,2,1:T(8,128)(2,1)S(1)} %bitcast.110), channel_id=1, source_target_pairs={{0,4},{4,8},{8,12},{1,5},{5,9},{9,13},{2,6},{6,10},{10,14},{3,7},{... | collective-permute-start | bytes 98312 | tf_op jit(solution)/shard_map/ppermute | solution.py:16
  45.0 0.0 copy-start.12
  45.0 3.7 %fusion.24 = bf16[768,512]{0,1:T(8,128)(2,1)S(1)} fusion(bf16[768,2048]{0,1:T(8,128)(2,1)S(1)} %bitcast.99, bf16[256,8,4,128]{3,2,1,0:T(4,128)(2,1)} %bitcast.114), kind=kOutput, calls=%fused_computation.30 | convolution fusion | flops 1611005952 | bytes 6029312 | tf_op jit(solution)/shard_map/dot_general | solution.py:89
  48.7 0.0 copy-start.11
  48.7 2.7 %convolution_convert_fusion = bf16[768,512]{1,0:T(8,128)(2,1)} fusion(bf16[768,2048]{0,1:T(8,128)(2,1)S(1)} %bitcast.100, bf16[2048,512]{0,1:T(8,128)(2,1)S(1)} %bitcast.115), kind=kOutput, calls=%fused_computation.31 | convolution fusion | flops 1611005952 | bytes 6029312 | tf_op jit(solution)/shard_map/dot_general | solution.py:80
  51.5 0.1 convert_reduce_fusion
  51.6 8.5 %all-gather.2 = f32[4,1,128]{2,1,0:T(1,128)S(1)} all-gather(f32[1,1,128]{2,1,0:T(1,128)S(1)} %bitcast.112), channel_id=3, replica_groups=mesh['grp'=2,'sp'=4,'fs'=2,'tp'=2] {'sp'}, dimensions={0}, use_global_device_ids=true | all-gather | bytes 2560 | tf_op jit(solution)/shard_map/all_gather | solution.py:103
  60.1 3.7 %collective-permute-start.2 = (bf16[128,4,128]{0,2,1:T(8,128)(2,1)S(1)}, bf16[128,4,128]{0,2,1:T(8,128)(2,1)}, u32[]{:S(2)}, u32[]{:S(2)}) collective-permute-start(bf16[128,4,128]{0,2,1:T(8,128)(2,1)S(1)} %bitcast.108), channel_id=1, source_target_pairs={{0,4},{4,8},{8,12},{1,5},{5,9},{9,13},{2,6},{6,10},{10,14},{3,7},{... | collective-permute-start | bytes 393224 | tf_op jit(solution)/shard_map/ppermute | solution.py:16
  63.7 0.6 select_reduce_fusion
  64.4 0.2 reshape.320
  64.7 3.6 %reshape.335 = bf16[6,128,2,4,64]{4,3,2,1,0:T(4,128)(2,1)} reshape(bf16[768,512]{1,0:T(8,128)(2,1)} %convolution_convert_fusion) | data formatting | bytes 1572864 | tf_op jit(solution)/shard_map/reshape | solution.py:31
  68.3 1.2 %concatenate.23 = f32[4,128]{1,0:T(4,128)} pad(f32[1,128]{1,0:T(1,128)} %bitcast.113, f32[]{:T(128)} %constant.14.clone.1), padding=3_0x0_0 | pad | bytes 2564 | tf_op jit(solution)/shard_map/concatenate | solution.py:120
  69.5 0.8 copy_bitcast_fusion
  70.3 2.7 %fusion.13 = (f32[6,2,4,128]{3,2,1,0:T(4,128)S(1)}, f32[6,2,256,128,4]{3,2,4,1,0:T(8,128)S(1)}) fusion(pred[6,128,256]{1,2,0:T(8,128)(4,1)S(1)} %broadcast_and_fusion, bf16[6,128,2,4,64]{4,3,2,1,0:T(4,128)(2,1)} %reshape.335, bf16[6,128,2,64]{1,3,2,0:T(8,128)(2,1)S(1)} %copy.30, bf16[6,128,2,64]{1,3,2,0:T(8,128)(2,1)S(1)} %copy_bitcast_fusion), kind=kOutput, calls=%fused_computation.19 | convolution fusion | flops 206825472 | bytes 7692288 | tf_op jit(solution)/shard_map/nqhgd,nkhd->nhgqk/dot_general | solution.py:49
  73.0 0.1 broadcast_maximum_fusion
  73.1 1.7 %fusion.8 = f32[6,2,4,128]{3,2,1,0:T(4,128)S(1)} fusion(f32[6,2,256,128,4]{3,2,4,1,0:T(8,128)S(1)} %get-tuple-element.6, f32[6,2,4,128]{3,2,1,0:T(4,128)S(1)} %broadcast_maximum_fusion, pred[6,128,256]{1,2,0:T(8,128)(4,1)S(1)} %broadcast_and_fusion), kind=kLoop, calls=%fused_computation.14 | loop fusion | flops 6285312 | bytes 6537216 | tf_op jit(solution)/shard_map/reduce_sum | solution.py:56
  74.7 0.1 exponential_add_fusion
  74.8 0.0 collective-permute-done
  74.8 0.8 copy_bitcast_fusion.1
  75.6 1.7 %fusion.30 = bf16[6,128,2,4,64]{1,4,3,2,0:T(8,128)(2,1)S(1)} fusion(f32[6,2,256,128,4]{3,2,4,1,0:T(8,128)S(1)} %get-tuple-element.6, f32[6,2,4,128]{3,2,1,0:T(4,128)S(1)} %exponential_add_fusion, f32[6,2,4,128]{3,2,1,0:T(4,128)S(1)} %broadcast_maximum_fusion, pred[6,128,256]{1,2,0:T(8,128)(4,1)S(1)} %broadcast_and_fusion, ...), kind=kOutput, calls=%fused_computation.34 | convolution fusion | flops 210370560 | bytes 7716864 | tf_op jit(solution)/shard_map/nhgqk,nkhd->nqhgd/dot_general | solution.py:58
  77.4 0.6 copy.34
  78.0 0.0 copy-start.10
  78.0 4.5 %fusion.37 = f32[768,2048]{1,0:T(8,128)} fusion(bf16[512,2048]{1,0:T(8,128)(2,1)S(1)} %bitcast.96, bf16[64,8,6,128]{3,2,1,0:T(8,128)(2,1)S(1)} %bitcast.101), kind=kOutput, calls=%fused_computation.40 | convolution fusion | flops 1610612736 | bytes 9175040 | tf_op jit(solution)/shard_map/dot_general | solution.py:131
  82.5 11.3 %fusion.7 = bf16[768,2048]{1,0:T(8,128)(2,1)} fusion(f32[768,2048]{1,0:T(8,128)} %fusion.37, bf16[4,128,2048]{2,1,0:T(8,128)(2,1)} %param.18, bf16[768,4,128]{0,2,1:T(8,128)(2,1)} %bitcast.107, f32[768,896]{1,0:T(8,128)} %subtract_convert_fusion, f32[4]{0:T(128)S(1)} %copy-done.10, pred[4,896]{1,0:T(4,128)(4,1)S(1)} %copy-done.8, ...), kind=kOutput, calls=%fused_computation.10 | convolution fusion | flops 2330460160 | bytes 15910416 | tf_op jit(solution)/shard_map/dot_general | solution.py:133
  93.8 0.0 reduce-scatter.2.cloned.1.call-update
  93.8 9.5 %reduce-scatter.2.cloned.1.call-done = bf16[384,2048]{1,0:T(8,128)(2,1)} async-done(((bf16[768,2048]{1,0:T(8,128)(2,1)}), bf16[384,2048]{1,0:T(8,128)(2,1)}) %reduce-scatter.2.cloned.1.call-update) | async-done | bytes 1572880 | tf_op jit(solution)/shard_map/reduce_scatter | solution.py:132
  (36 shorter events, 0.2 us)
Async XLA Ops:
  6.5 71.4 %copy-start = (bf16[8,64,2048]{2,1,0:T(8,128)(2,1)S(1)}, bf16[8,64,2048]{2,1,0:T(8,128)(2,1)}, u32[]{:S(2)}) copy-start(bf16[8,64,2048]{2,1,0:T(8,128)(2,1)} %param.17) | copy-start | bytes 6291460
  6.5 17.2 %all-gather.5.cloned.1.call-start = ((), (), s32[]{:S(2)}) async-start(), calls=%async_computation.2 | async-start | bytes 4718592 | tf_op jit(solution)/shard_map/all_gather | solution.py:9
  7.3 96.0 %reduce-scatter.2.cloned.1.call-start = ((), (), s32[]{:S(2)}) async-start(), calls=%async_computation.1 | async-start | bytes 4718592 | tf_op jit(solution)/shard_map/reduce_scatter | solution.py:132
  28.4 2.8 %copy-start.1 = (bf16[2,768,1024]{1,2,0:T(8,128)(2,1)S(1)}, bf16[2,768,1024]{1,2,0:T(8,128)(2,1)}, u32[]{:S(2)}) copy-start(bf16[2,768,1024]{1,2,0:T(8,128)(2,1)} %copy.26) | copy-start | bytes 9437188
  31.2 2.4 %copy-start.5 = (bf16[2048,2,64]{0,2,1:T(8,128)(2,1)S(1)}, bf16[2048,2,64]{0,2,1:T(8,128)(2,1)}, u32[]{:S(2)}) copy-start(bf16[2048,2,64]{0,2,1:T(8,128)(2,1)} %param.14) | copy-start | bytes 1572868
  32.0 1.7 %copy-start.2 = (bf16[2,1,768,1024]{2,3,0,1:T(8,128)(2,1)}, bf16[2,1,768,1024]{2,3,0,1:T(8,128)(2,1)S(1)}, u32[]{:S(2)}) copy-start(bf16[2,1,768,1024]{2,3,0,1:T(8,128)(2,1)S(1)} %fusion.6) | copy-start | bytes 9437188
  32.0 7.0 %copy-start.6 = (bf16[2048,2,64]{0,2,1:T(8,128)(2,1)S(1)}, bf16[2048,2,64]{0,2,1:T(8,128)(2,1)}, u32[]{:S(2)}) copy-start(bf16[2048,2,64]{0,2,1:T(8,128)(2,1)} %param.13) | copy-start | bytes 1572868
  34.5 10.5 %copy-start.3 = (bf16[2,1,768,1024]{2,3,0,1:T(8,128)(2,1)S(1)}, bf16[2,1,768,1024]{2,3,0,1:T(8,128)(2,1)}, u32[]{:S(2)}) copy-start(bf16[2,1,768,1024]{2,3,0,1:T(8,128)(2,1)} %copy-done.2) | copy-start | bytes 9437188
  34.5 40.3 %collective-permute-start = (bf16[128,2,64]{0,2,1:T(8,128)(2,1)S(1)}, bf16[128,2,64]{0,2,1:T(8,128)(2,1)}, u32[]{:S(2)}, u32[]{:S(2)}) collective-permute-start(bf16[128,2,64]{0,2,1:T(8,128)(2,1)S(1)} %bitcast.109), channel_id=1, source_target_pairs={{0,4},{4,8},{8,12},{1,5},{5,9},{9,13},{2,6},{6,10},{10,14},{3,7},{... | collective-permute-start | bytes 98312 | tf_op jit(solution)/shard_map/ppermute | solution.py:16
  41.5 28.0 %collective-permute-start.1 = (bf16[128,2,64]{0,2,1:T(8,128)(2,1)S(1)}, bf16[128,2,64]{0,2,1:T(8,128)(2,1)}, u32[]{:S(2)}, u32[]{:S(2)}) collective-permute-start(bf16[128,2,64]{0,2,1:T(8,128)(2,1)S(1)} %bitcast.110), channel_id=1, source_target_pairs={{0,4},{4,8},{8,12},{1,5},{5,9},{9,13},{2,6},{6,10},{10,14},{3,7},{... | collective-permute-start | bytes 98312 | tf_op jit(solution)/shard_map/ppermute | solution.py:16
  45.0 3.7 %copy-start.12 = (bf16[2048,8,64]{0,2,1:T(8,128)(2,1)S(1)}, bf16[2048,8,64]{0,2,1:T(8,128)(2,1)}, u32[]{:S(2)}) copy-start(bf16[2048,8,64]{0,2,1:T(8,128)(2,1)} %param.12) | copy-start | bytes 6291460
  48.7 2.8 %copy-start.7 = (bf16[768,512]{0,1:T(8,128)(2,1)}, bf16[768,512]{0,1:T(8,128)(2,1)S(1)}, u32[]{:S(2)}) copy-start(bf16[768,512]{0,1:T(8,128)(2,1)S(1)} %fusion.24) | copy-start | bytes 2359300
  48.7 15.0 %copy-start.11 = (pred[4]{0:T(512)(128)(4,1)S(1)}, pred[4]{0:T(512)(128)(4,1)}, u32[]{:S(2)}) copy-start(pred[4]{0:T(512)(128)(4,1)} %iota_compare_fusion.1) | copy-start | bytes 16
  60.1 22.4 %collective-permute-start.2 = (bf16[128,4,128]{0,2,1:T(8,128)(2,1)S(1)}, bf16[128,4,128]{0,2,1:T(8,128)(2,1)}, u32[]{:S(2)}, u32[]{:S(2)}) collective-permute-start(bf16[128,4,128]{0,2,1:T(8,128)(2,1)S(1)} %bitcast.108), channel_id=1, source_target_pairs={{0,4},{4,8},{8,12},{1,5},{5,9},{9,13},{2,6},{6,10},{10,14},{3,7},{... | collective-permute-start | bytes 393224 | tf_op jit(solution)/shard_map/ppermute | solution.py:16
  77.9 4.5 %copy-start.4 = (pred[768,896]{1,0:T(8,128)(4,1)S(1)}, pred[768,896]{1,0:T(8,128)(4,1)}, u32[]{:S(2)}) copy-start(pred[768,896]{1,0:T(8,128)(4,1)} %broadcast_compare_fusion) | copy-start | bytes 2064388
  78.0 4.5 %copy-start.8 = (pred[4,896]{1,0:T(4,128)(4,1)S(1)}, pred[4,896]{1,0:T(4,128)(4,1)}, u32[]{:S(2)}) copy-start(pred[4,896]{1,0:T(4,128)(4,1)} %broadcast_or_fusion) | copy-start | bytes 10756
  78.0 4.5 %copy-start.9 = (f32[4,128]{1,0:T(4,128)S(1)}, f32[4,128]{1,0:T(4,128)}, u32[]{:S(2)}) copy-start(f32[4,128]{1,0:T(4,128)} %concatenate.23) | copy-start | bytes 6148
  78.0 4.5 %copy-start.10 = (f32[4]{0:T(128)S(1)}, f32[4]{0:T(128)}, u32[]{:S(2)}) copy-start(f32[4]{0:T(128)} %constant.13.clone) | copy-start | bytes 52
Sparse Core Ops, SparseCore 0:
  8.9 14.8 all-gather.4
  94.0 9.2 reduce-scatter.1
